TPU v7x, 128 devices: a whole 4x4x4 slice. The times are simulated.
128 devices in a mesh: rep: 2 (over z_hi), fs: 32 (over z_lo, y, x), tp: 2 (over core).
Axes of the slice: x: 4, y: 4, z: 4 (z_hi: 2, z_lo: 2; z = z_hi * 2 + z_lo), core: 2. Of those that a mesh axis runs over, the one named last changes fastest.
Arguments:
- tokens: bfloat16 [65536, 2048], P(('rep', 'fs', 'tp')), parts along dimension 0, may hold values from -6 to 6
- mix_gain: float32 [2048], replicated, may hold values from 0.1 to 1.9
- w_query: bfloat16 [2048, 512], P('fs', 'tp'), may hold values from -0.125 to 0.125
- w_key: bfloat16 [2048, 512], P('fs', 'tp'), may hold values from -0.125 to 0.125
- w_value: bfloat16 [2048, 1024], P('fs', 'tp'), may hold values from -0.125 to 0.125
- w_out: bfloat16 [1024, 2048], P('tp', 'fs'), may hold values from -0.1875 to 0.1875
- ffn_gain: float32 [2048], replicated, may hold values from 0.1 to 1.9
- w_ffgate: bfloat16 [2048, 2816], P('fs', 'tp'), may hold values from -0.125 to 0.125
- w_ffup: bfloat16 [2048, 2816], P('fs', 'tp'), may hold values from -0.125 to 0.125
- conv_gate: float32 [3, 2816], replicated, may hold values from -3 to 3
- conv_up: float32 [3, 2816], replicated, may hold values from -3 to 3
- w_down: bfloat16 [2816, 2048], P('tp', 'fs'), may hold values from -0.109375 to 0.109375
Outputs:
- layer_out: bfloat16 [65536, 2048], P(('rep', 'fs', 'tp')), parts along dimension 0
There are 2 independent parts, one for each index of `rep`. A program takes and returns all parts, laid end to end along the dimension named above; an argument that names none is the same for every part. Nothing has to cross between parts.
All inputs are finite; a program needn't handle non-finite values.
Results may differ from a plain program's by a relative error of at most 0.014.
Values may be sent and summed in bfloat16 or wider, within the bound.
No kernel may reach another device: no remote copies, remote signals or barrier semaphores. Data moves between devices by JAX's collectives and lax.ppermute only.
A program may use at most 128 MiB of HBM per device.

v0:
```python
import jax
import jax.numpy as jnp
from jax import lax
from jax.sharding import PartitionSpec as P

HEADS = 4
DK = 128
DV = 256
KERNEL = 3
BLOCK = 128
LENGTH = 1024
epsilon = 1e-06


def in_one_piece(arrays, axis, dim, along):
    both = jnp.concatenate(arrays, axis=along)
    out, at, done = (lax.all_gather(both, axis, axis=dim, tiled=True), 0, [])
    for a in arrays:
        done.append(lax.slice_in_dim(out, at, at + a.shape[along], axis=along))
        at += a.shape[along]
    return tuple(done)


def copy_for_each(shard, axis):
    length = lax.axis_size(axis)
    return lax.all_to_all(
        jnp.broadcast_to(shard[None], (length, *shard.shape)), axis, 0, 0, tiled=True
    )


def in_order(pieces, dim):
    pieces = jnp.moveaxis(pieces, 0, dim)
    dims = pieces.shape
    return pieces.reshape(*dims[:dim], dims[dim] * dims[dim + 1], *dims[dim + 2 :])


def collect(shard, axis, dim):
    pieces = copy_for_each(shard, axis)
    return in_order(pieces, dim)


def in_blocks(shard, dim, length):
    dims = shard.shape
    pieces = shard.reshape(*dims[:dim], length, dims[dim] // length, *dims[dim + 1 :])
    return jnp.moveaxis(pieces, dim, 0)


def sent_and_summed(shard, axis, dim):
    length = lax.axis_size(axis)
    pieces = lax.all_to_all(in_blocks(shard, dim, length), axis, 0, 0, tiled=True)
    return jnp.sum(pieces.astype(jnp.float32), axis=0)


def rms_rows(matrix, scale_vec):
    values = matrix.astype(jnp.float32)
    factor = lax.rsqrt(jnp.mean(values * values, axis=-1, keepdims=True) + epsilon)
    return (values * factor * scale_vec).astype(jnp.bfloat16)


def rotate_heads(matrix):
    length = matrix.shape[0]
    half_width = matrix.shape[-1] // 2
    inverse = 10000.0 ** (-jnp.arange(half_width, dtype=jnp.float32) * 2.0 / (2 * half_width))
    angles = jnp.arange(length, dtype=jnp.float32)[:, None] * inverse[None, :]
    cosine = jnp.cos(angles)[:, None, :]
    sine = jnp.sin(angles)[:, None, :]
    values = matrix.astype(jnp.float32)
    first_half = values[..., :half_width]
    second_half = values[..., half_width:]
    return jnp.concatenate(
        [first_half * cosine - second_half * sine, first_half * sine + second_half * cosine],
        axis=-1,
    )


def retain_blocks(rot_query, rot_key, value, rates, block_len):
    length, head_count, width_k = rot_query.shape
    width_v = value.shape[-1]
    blocks = length // block_len
    query4 = rot_query.reshape(blocks, block_len, head_count, width_k)
    key4 = rot_key.reshape(blocks, block_len, head_count, width_k)
    value4 = value.reshape(blocks, block_len, head_count, width_v)
    places = jnp.arange(block_len, dtype=jnp.float32)
    spacing = places[:, None] - places[None, :]
    inside = jnp.where(
        spacing[None] >= 0, jnp.exp(-jnp.maximum(spacing, 0.0)[None] * rates[:, None, None]), 0.0
    )
    scores = jnp.einsum("cihd,cjhd->chij", query4, key4, preferred_element_type=jnp.float32)
    weights = (scores * inside[None]).astype(jnp.bfloat16)
    inner_part = jnp.einsum("chij,cjhe->cihe", weights, value4, preferred_element_type=jnp.float32)
    tail_decay = jnp.exp(-(block_len - 1.0 - places)[:, None] * rates[None, :])
    decayed = (key4.astype(jnp.float32) * tail_decay[None, :, :, None]).astype(jnp.bfloat16)
    states = jnp.einsum("cjhd,cjhe->chde", decayed, value4, preferred_element_type=jnp.float32)
    passing = jnp.exp(-block_len * rates)[:, None, None]

    def advance(carried, fresh):
        return (carried * passing + fresh, carried)

    _, before = lax.scan(advance, jnp.zeros((head_count, width_k, width_v), jnp.float32), states)
    onset_decay = jnp.exp(-(places + 1.0)[:, None] * rates[None, :])
    cross_part = (
        jnp.einsum("cihd,chde->cihe", query4.astype(jnp.float32), before)
        * onset_decay[None, :, :, None]
    )
    return (inner_part + cross_part).reshape(length, head_count, width_v)


def head_norm(retained):
    average = jnp.mean(retained, axis=-1, keepdims=True)
    centered = retained - average
    return centered * lax.rsqrt(jnp.mean(centered * centered, axis=-1, keepdims=True) + epsilon)


def causal_taps(matrix, kernel_w):
    length = matrix.shape[0]
    padded = jnp.pad(matrix.astype(jnp.float32), ((KERNEL - 1, 0), (0, 0)))
    total = jnp.zeros((length, matrix.shape[1]), jnp.float32)
    for tap_idx in range(KERNEL):
        total = total + kernel_w[tap_idx][None, :] * padded[tap_idx : tap_idx + length]
    return total


def collect_ffn(w_ffgate, w_ffup):
    return in_one_piece((w_ffgate, w_ffup), "fs", 0, 1)


def body(
    tokens,
    mix_gain,
    w_query,
    w_key,
    w_value,
    w_out,
    ffn_gain,
    w_ffgate,
    w_ffup,
    conv_gate,
    conv_up,
    w_down,
):
    tp_rank = lax.axis_index("tp")
    heads_here = w_query.shape[1] // DK
    ffn_pair = None
    normed = rms_rows(tokens, mix_gain)
    query_w, key_w, value_w = in_one_piece((w_query, w_key, w_value), "fs", 0, 1)
    qk_cols = query_w.shape[1]
    pieces = lax.all_gather(normed, "tp", axis=0, tiled=True)
    joined = jnp.concatenate(
        [
            jnp.dot(pieces, query_w, preferred_element_type=jnp.float32),
            jnp.dot(pieces, key_w, preferred_element_type=jnp.float32),
            jnp.dot(pieces, value_w, preferred_element_type=jnp.float32),
        ],
        axis=1,
    ).astype(jnp.bfloat16)
    length = joined.shape[0]
    query = joined[:, :qk_cols].reshape(length, heads_here, DK)
    key = joined[:, qk_cols : 2 * qk_cols].reshape(length, heads_here, DK)
    value = joined[:, 2 * qk_cols :].reshape(length, heads_here, DV)
    rot_query = rotate_heads(query).astype(jnp.bfloat16)
    rot_key = (rotate_heads(key) * DK ** (-0.5)).astype(jnp.bfloat16)
    head_ids = (tp_rank * heads_here + jnp.arange(heads_here, dtype=jnp.int32)).astype(jnp.float32)
    rates = 1.0 / 16.0 * (32.0 / LENGTH) ** (head_ids / (HEADS - 1))
    retained = retain_blocks(rot_query, rot_key, value, rates, BLOCK)
    hidden = head_norm(retained).reshape(length, heads_here * DV).astype(jnp.bfloat16)
    out_full = collect(w_out, "fs", 1)
    mix_sum = sent_and_summed(
        jnp.dot(hidden, out_full, preferred_element_type=jnp.float32).astype(jnp.bfloat16), "tp", 0
    )
    resid = (tokens.astype(jnp.float32) + mix_sum).astype(jnp.bfloat16)
    normed_ffn = rms_rows(resid, ffn_gain)
    ff_here = w_ffgate.shape[1]
    ffn_pair = collect_ffn(w_ffgate, w_ffup)
    gate_w, up_w = ffn_pair
    pieces = lax.all_gather(normed_ffn, "tp", axis=0, tiled=True)
    both_pre = jnp.concatenate(
        [
            jnp.dot(pieces, gate_w, preferred_element_type=jnp.float32),
            jnp.dot(pieces, up_w, preferred_element_type=jnp.float32),
        ],
        axis=1,
    ).astype(jnp.bfloat16)
    gate_pre = both_pre[:, :ff_here]
    up_pre = both_pre[:, ff_here:]
    gate_taps = lax.dynamic_slice_in_dim(conv_gate, tp_rank * ff_here, ff_here, 1)
    up_taps = lax.dynamic_slice_in_dim(conv_up, tp_rank * ff_here, ff_here, 1)
    activ = (jax.nn.silu(causal_taps(gate_pre, gate_taps)) * causal_taps(up_pre, up_taps)).astype(
        jnp.bfloat16
    )
    down_full = lax.all_gather(w_down, "fs", axis=1, tiled=True)
    ffn_sum = sent_and_summed(
        jnp.dot(activ, down_full, preferred_element_type=jnp.float32).astype(jnp.bfloat16), "tp", 0
    )
    return (resid.astype(jnp.float32) + ffn_sum).astype(jnp.bfloat16)


def solution(mesh):
    placed = (
        P(("rep", "fs", "tp"), None),
        P(),
        P("fs", "tp"),
        P("fs", "tp"),
        P("fs", "tp"),
        P("tp", "fs"),
        P(),
        P("fs", "tp"),
        P("fs", "tp"),
        P(),
        P(),
        P("tp", "fs"),
    )
    return jax.shard_map(
        body, mesh=mesh, in_specs=placed, out_specs=P(("rep", "fs", "tp"), None), check_vma=False
    )
```

profile of v0, /device:TPU:1, one launch (start us, length us, event | category | flops | bytes accessed | tf_op | source)
XLA Modules:
  0.0 637.9 jit_solution(8390424234193751009)
XLA Ops:
  6.6 2.1 fusion.6
  8.7 3.5 fusion.8
  12.3 0.7 pad_maximum_fusion.2
  13.0 1.5 broadcast_in_dim.25
  14.5 9.3 %all-to-all-start = ((bf16[32,512,64]{1,2,0:T(8,128)(2,1)}), bf16[32,512,64]{1,2,0:T(8,128)(2,1)}, u32[]{:S(2)}, u32[]{:S(2)}) async-start(bf16[32,512,64]{1,2,0:T(8,128)(2,1)} %broadcast_in_dim.25), calls=%async_computation | async-start | bytes 4194304 | tf_op jit(solution)/shard_map/all_to_all | solution.py:26
  24.2 1.0 fusion.44
  25.2 7.1 %all-gather.6.cloned.1.call-done = bf16[1024,2048]{1,0:T(8,128)(2,1)} async-done(((bf16[512,2048]{1,0:T(8,128)(2,1)}), bf16[1024,2048]{1,0:T(8,128)(2,1)}) %all-gather.6.cloned.1.call-update) | async-done | bytes 4194320 | tf_op jit(solution)/shard_map/all_gather | solution.py:147
  32.3 140.7 %all-gather.8.cloned.1.call-done = bf16[2048,1024]{1,0:T(8,128)(2,1)} async-done(((bf16[64,1024]{1,0:T(8,128)(2,1)}), bf16[2048,1024]{1,0:T(8,128)(2,1)}) %all-gather.8.cloned.1.call-update) | async-done | bytes 4194320 | tf_op jit(solution)/shard_map/all_gather | solution.py:17
  173.0 3.9 convolution_convert_fusion.3
  177.1 2.5 convolution_convert_fusion.2
  179.7 1.1 subtract_convert_fusion
  181.8 6.2 fusion.31
  187.9 1.3 reshape_reshape.3
  189.6 0.8 copy-done.1
  190.4 0.6 fusion.38
  191.0 6.5 %while.13 = (s32[]{:T(128)}, f32[2,128,256]{2,1,0:T(8,128)S(1)}, bf16[8,2,128,256]{3,2,1,0:T(8,128)(2,1)}, f32[8,2,128,256]{3,2,1,0:T(8,128)S(1)}, s32[]{:T(128)}, /*index=5*/s32[]{:T(128)}, s32[]{:T(128)}) while((s32[]{:T(128)}, f32[2,128,256]{2,1,0:T(8,128)S(1)}, bf16[8,2,128,256]{3,2,1,0:T(8,128)(2,1)}, ...), condition=%wide.region_2.3_spmd.clone, body=%wide.region_1.2_spmd.clone.sunk | while | flops 262155 | bytes 1180272 | solution.py:99
  191.0 0.7 bitcast_dynamic-update-slice_fusion.2
  191.8 0.7 bitcast_dynamic-update-slice_fusion.2
  192.6 0.7 bitcast_dynamic-update-slice_fusion.2
  193.4 0.7 bitcast_dynamic-update-slice_fusion.2
  194.3 0.7 bitcast_dynamic-update-slice_fusion.2
  195.1 0.7 bitcast_dynamic-update-slice_fusion.2
  195.9 0.7 bitcast_dynamic-update-slice_fusion.2
  196.7 0.7 bitcast_dynamic-update-slice_fusion.2
  197.5 1.0 copy.48
  198.8 1.2 copy.49
  200.3 3.2 fusion.45
  203.6 3.0 fusion.54
  206.8 0.7 multiply_reduce_fusion
  207.5 0.9 fusion.29
  208.3 0.5 copy.46
  208.9 4.0 convolution_convert_fusion.1
  212.9 27.5 %all_to_all.15 = bf16[2,512,2048]{2,1,0:T(8,128)(2,1)S(1)} all-to-all(bf16[2,512,2048]{2,1,0:T(8,128)(2,1)S(1)} %bitcast.73), channel_id=1, replica_groups=mesh['rep'=2,'fs'=32,'tp'=2] {'tp'}, dimensions={0} | all-to-all | bytes 8388608 | tf_op jit(solution)/shard_map/all_to_all | solution.py:50
  240.4 1.0 convert_reduce_fusion.1
  241.3 0.6 copy-done
  241.9 0.7 fusion.10
  242.7 1.9 fusion.12
  244.6 0.8 pad_maximum_fusion.1
  246.0 1.1 dynamic-slice_reduce_fusion.2
  247.1 15.1 %all-gather.10.cloned.1.call-done = bf16[1024,2048]{1,0:T(8,128)(2,1)} async-done(((bf16[512,2048]{1,0:T(8,128)(2,1)}), bf16[1024,2048]{1,0:T(8,128)(2,1)}) %all-gather.10.cloned.1.call-update) | async-done | bytes 4194320 | tf_op jit(solution)/shard_map/all_gather | solution.py:175
  262.2 155.1 %all-gather.12.cloned.1.call-done = bf16[2048,2816]{1,0:T(8,128)(2,1)} async-done(((bf16[64,2816]{1,0:T(8,128)(2,1)}), bf16[2048,2816]{1,0:T(8,128)(2,1)}) %all-gather.12.cloned.1.call-update) | async-done | bytes 11534352 | tf_op jit(solution)/shard_map/all_gather | solution.py:17
  417.3 11.8 %fusion.17 = f32[1024,1408]{1,0:T(8,128)} fusion(bf16[1024,2048]{1,0:T(8,128)(2,1)} %all-gather.10.cloned.1.call-done, bf16[2048,2816]{1,0:T(8,128)(2,1)} %all-gather.12.cloned.1.call-done), kind=kOutput, calls=%fused_computation.26 | convolution fusion | flops 5908463616 | bytes 15728640 | tf_op jit(solution)/shard_map/dot_general | solution.py:178
  429.1 8.5 %fusion.23 = f32[1024,1408]{1,0:T(8,128)} fusion(bf16[1024,2048]{1,0:T(8,128)(2,1)S(1)} %copy-done.13, bf16[2048,2816]{1,0:T(8,128)(2,1)S(1)} %copy-done.11), kind=kOutput, calls=%fused_computation.28 | convolution fusion | flops 5908463616 | bytes 15728640 | tf_op jit(solution)/shard_map/dot_general | solution.py:179
  437.6 139.5 %all-gather.14.cloned.1.call-done = bf16[1408,2048]{0,1:T(8,128)(2,1)} async-done(((bf16[1408,64]{0,1:T(8,128)(2,1)}), bf16[1408,2048]{0,1:T(8,128)(2,1)}) %all-gather.14.cloned.1.call-update) | async-done | bytes 5767184 | tf_op jit(solution)/shard_map/all_gather | solution.py:190
  577.1 23.0 %convolution_convert_fusion = bf16[1024,2048]{1,0:T(8,128)(2,1)} fusion(bf16[1408,2048]{0,1:T(8,128)(2,1)} %all-gather.14.cloned.1.call-done, f32[1024,1408]{1,0:T(8,128)} %fusion.23, f32[1024,1408]{1,0:T(8,128)} %fusion.17, f32[1408]{0:T(1024)S(1)} %get-tuple-element.59, f32[1408]{0:T(1024)S(1)} %get-tuple-element.58, f32[1408]{0:T(1024)S(1)} %get-tuple-element.57, ...), kind=kOutput, calls=%fused_computation.29 | convolution fusion | flops 5930745856 | bytes 21529600 | tf_op jit(solution)/shard_map/dot_general | solution.py:192
  600.1 28.2 %all_to_all.16 = bf16[2,512,2048]{2,1,0:T(8,128)(2,1)S(1)} all-to-all(bf16[2,512,2048]{2,1,0:T(8,128)(2,1)} %bitcast.72), channel_id=1, replica_groups=mesh['rep'=2,'fs'=32,'tp'=2] {'tp'}, dimensions={0} | all-to-all | bytes 8388608 | tf_op jit(solution)/shard_map/all_to_all | solution.py:50
  628.3 1.0 convert_reduce_fusion
  629.3 2.1 fusion.13
  (76 shorter events, 4.3 us)
Async XLA Ops:
  6.5 5.7 copy-start.7
  6.5 5.7 copy-start.8
  6.5 5.7 copy-start.9
  6.5 6.4 %copy-start.6 = (bf16[512,64]{0,1:T(8,128)(2,1)S(1)}, bf16[512,64]{0,1:T(8,128)(2,1)}, u32[]{:S(2)}) copy-start(bf16[512,64]{0,1:T(8,128)(2,1)} %param.19) | copy-start | bytes 196612
  6.5 25.8 %all-gather.6.cloned.1.call-start = ((), (), s32[]{:S(2)}) async-start(), calls=%async_computation.3 | async-start | bytes 6291456 | tf_op jit(solution)/shard_map/all_gather | solution.py:147
  12.2 160.8 %all-gather.8.cloned.1.call-start = ((), (), s32[]{:S(2)}) async-start(), calls=%async_computation.4 | async-start | bytes 4325376 | tf_op jit(solution)/shard_map/all_gather | solution.py:17
  14.5 194.4 %all-to-all-start = ((bf16[32,512,64]{1,2,0:T(8,128)(2,1)}), bf16[32,512,64]{1,2,0:T(8,128)(2,1)}, u32[]{:S(2)}, u32[]{:S(2)}) async-start(bf16[32,512,64]{1,2,0:T(8,128)(2,1)} %broadcast_in_dim.25), calls=%async_computation | async-start | bytes 4194304 | tf_op jit(solution)/shard_map/all_to_all | solution.py:26
  23.9 238.3 %all-gather.10.cloned.1.call-start = ((), (), s32[]{:S(2)}) async-start(), calls=%async_computation.5 | async-start | bytes 6291456 | tf_op jit(solution)/shard_map/all_gather | solution.py:175
  173.0 4.1 copy-start.12
  189.6 0.8 copy-start.1
  198.8 4.8 copy-start.2
  200.3 3.2 copy-start.3
  240.4 1.6 copy-start
  241.9 0.7 copy-start.10
  242.6 2.0 copy-start.4
  242.6 2.0 copy-start.5
  244.6 172.7 %all-gather.12.cloned.1.call-start = ((), (), s32[]{:S(2)}) async-start(), calls=%async_computation.6 | async-start | bytes 11894784 | tf_op jit(solution)/shard_map/all_gather | solution.py:17
  245.4 331.7 %all-gather.14.cloned.1.call-start = ((), (), s32[]{:S(2)}) async-start(), calls=%async_computation.7 | async-start | bytes 5947392 | tf_op jit(solution)/shard_map/all_gather | solution.py:190
  417.3 11.8 %copy-start.11 = (bf16[2048,2816]{1,0:T(8,128)(2,1)S(1)}, bf16[2048,2816]{1,0:T(8,128)(2,1)}, u32[]{:S(2)}) copy-start(bf16[2048,2816]{1,0:T(8,128)(2,1)} %all-gather.12.cloned.1.call-done) | copy-start | bytes 34603012
  417.3 11.9 %copy-start.13 = (bf16[1024,2048]{1,0:T(8,128)(2,1)S(1)}, bf16[1024,2048]{1,0:T(8,128)(2,1)}, u32[]{:S(2)}) copy-start(bf16[1024,2048]{1,0:T(8,128)(2,1)} %all-gather.10.cloned.1.call-done) | copy-start | bytes 12582916
Sparse Core Ops, SparseCore 0:
  12.3 19.9 all-gather.5
  34.0 138.9 all-gather.7
  244.7 17.4 all-gather.9
  263.7 153.5 all-gather.11
  418.8 158.2 all-gather.13
where the time goes:
time: 639 us; the launch traced here: 638 us
  waiting for transfers between devices  458 us (72%)
  matrix products  66.7 us (10%)
  blocking collectives  55.7 us (9%)
  other arithmetic  24.3 us (4%)
  between operations  13.5 us (2%)
  local copies, waits for them, and re-layouts  9.83 us (2%)
  starting transfers between devices  9.54 us (1%)
    all_gather x2, waiting for transfers between devices, in_one_piece(): out, at, done = (lax.all_gather(both, axis, axis=dim, tiled=True), 0, [])  296 us
    all_gather x1, waiting for transfers between devices, body(): down_full = lax.all_gather(w_down, 'fs', axis=1, tiled=True)  139 us
    all_to_all x2, blocking collectives, sent_and_summed(): lax.all_to_all(in_blocks(shard, dim, length), axis, 0, 0, tiled=True)  55.7 us
    dot_general x1, matrix products, body(): jnp.dot(activ, down_full, preferred_element_type=jnp.float32)  23 us
    all_gather x1, waiting for transfers between devices, body(): pieces = lax.all_gather(normed_ffn, 'tp', axis=0, tiled=True)  15.1 us
  transfers between devices with their start and end apart: 6, of which 5 were waited for; matrix products, arithmetic and copies ran while one was open for 9% of the time, Pallas kernels for 0%

commit v1 on v0

--- a/solution.py
+++ b/solution.py
@@ -187,7 +187,7 @@
     activ = (jax.nn.silu(causal_taps(gate_pre, gate_taps)) * causal_taps(up_pre, up_taps)).astype(
         jnp.bfloat16
     )
-    down_full = lax.all_gather(w_down, "fs", axis=1, tiled=True)
+    down_full = jnp.concatenate(lax.all_gather(w_down, "fs"), axis=1)
     ffn_sum = sent_and_summed(
         jnp.dot(activ, down_full, preferred_element_type=jnp.float32).astype(jnp.bfloat16), "tp", 0
     )

time: 639 us -> 611 us (0.956)
  waiting for transfers between devices: 458 us -> 423 us
  local copies, waits for them, and re-layouts: 9.83 us -> 17.8 us
    all_gather x1, waiting for transfers between devices: 139 us -> 90.2 us  [body(): down_full = jnp.concatenate(lax.all_gather(w_down, 'fs'), axis=1)]
    all_gather x1, waiting for transfers between devices: 15.1 us -> 30 us  [body(): pieces = lax.all_gather(normed_ffn, 'tp', axis=0, tiled=True)]
where the time goes in v1:
time: 611 us
  waiting for transfers between devices  423 us (69%)
  matrix products  66.8 us (11%)
  blocking collectives  55.6 us (9%)
  other arithmetic  24.4 us (4%)
  local copies, waits for them, and re-layouts  17.8 us (3%)
  between operations  13.6 us (2%)
  starting transfers between devices  9.76 us (2%)
    all_gather x2, waiting for transfers between devices, in_one_piece(): out, at, done = (lax.all_gather(both, axis, axis=dim, tiled=True), 0, [])  295 us
    all_gather x1, waiting for transfers between devices, body(): down_full = jnp.concatenate(lax.all_gather(w_down, 'fs'), axis=1)  90.2 us
    all_to_all x2, blocking collectives, sent_and_summed(): lax.all_to_all(in_blocks(shard, dim, length), axis, 0, 0, tiled=True)  55.6 us
    all_gather x1, waiting for transfers between devices, body(): pieces = lax.all_gather(normed_ffn, 'tp', axis=0, tiled=True)  30 us
    dot_general x1, matrix products, body(): jnp.dot(activ, down_full, preferred_element_type=jnp.float32)  23 us
  transfers between devices with their start and end apart: 6, of which 5 were waited for; matrix products, arithmetic and copies ran while one was open for 9% of the time, Pallas kernels for 0%

profile of v1, /device:TPU:1, one launch (start us, length us, event | category | flops | bytes accessed | tf_op | source)
XLA Modules:
  0.0 610.7 jit_solution(13414776563466217259)
XLA Ops:
  6.6 2.1 fusion.6
  8.7 3.5 fusion.8
  12.3 0.7 pad_maximum_fusion.2
  13.0 1.6 broadcast_in_dim.25
  14.6 9.3 %all-to-all-start = ((bf16[32,512,64]{1,2,0:T(8,128)(2,1)}), bf16[32,512,64]{1,2,0:T(8,128)(2,1)}, u32[]{:S(2)}, u32[]{:S(2)}) async-start(bf16[32,512,64]{1,2,0:T(8,128)(2,1)} %broadcast_in_dim.25), calls=%async_computation | async-start | bytes 4194304 | tf_op jit(solution)/shard_map/all_to_all | solution.py:26
  23.9 0.7 all-gather.15.cloned.1.call-update
  25.0 1.0 fusion.44
  26.0 6.3 %all-gather.7.cloned.1.call-done = bf16[1024,2048]{1,0:T(8,128)(2,1)} async-done(((bf16[512,2048]{1,0:T(8,128)(2,1)}), bf16[1024,2048]{1,0:T(8,128)(2,1)}) %all-gather.7.cloned.1.call-update) | async-done | bytes 4194320 | tf_op jit(solution)/shard_map/all_gather | solution.py:147
  32.3 140.2 %all-gather.9.cloned.1.call-done = bf16[2048,1024]{1,0:T(8,128)(2,1)} async-done(((bf16[64,1024]{1,0:T(8,128)(2,1)}), bf16[2048,1024]{1,0:T(8,128)(2,1)}) %all-gather.9.cloned.1.call-update) | async-done | bytes 4194320 | tf_op jit(solution)/shard_map/all_gather | solution.py:17
  172.6 3.9 convolution_convert_fusion.3
  176.6 2.5 convolution_convert_fusion.2
  179.3 1.1 subtract_convert_fusion
  181.3 6.2 %fusion.31 = bf16[1024,512]{1,0:T(8,128)(2,1)} fusion(bf16[1024,2048]{1,0:T(8,128)(2,1)} %all-gather.7.cloned.1.call-done, bf16[2048,1024]{1,0:T(8,128)(2,1)} %all-gather.9.cloned.1.call-done), kind=kOutput, calls=%fused_computation.39 | convolution fusion | flops 2148007936 | bytes 7340032 | tf_op jit(solution)/shard_map/dot_general | solution.py:152
  187.5 1.3 reshape_reshape.3
  189.2 0.8 copy-done.1
  190.5 6.5 %while.13 = (s32[]{:T(128)}, f32[2,128,256]{2,1,0:T(8,128)S(1)}, bf16[8,2,128,256]{3,2,1,0:T(8,128)(2,1)}, f32[8,2,128,256]{3,2,1,0:T(8,128)S(1)}, s32[]{:T(128)}, /*index=5*/s32[]{:T(128)}, s32[]{:T(128)}) while((s32[]{:T(128)}, f32[2,128,256]{2,1,0:T(8,128)S(1)}, bf16[8,2,128,256]{3,2,1,0:T(8,128)(2,1)}, ...), condition=%wide.region_2.3_spmd.clone, body=%wide.region_1.2_spmd.clone.sunk | while | flops 262155 | bytes 1180272 | solution.py:99
  190.5 0.7 bitcast_dynamic-update-slice_fusion.2
  191.4 0.7 bitcast_dynamic-update-slice_fusion.2
  192.2 0.7 bitcast_dynamic-update-slice_fusion.2
  193.0 0.7 bitcast_dynamic-update-slice_fusion.2
  193.8 0.7 bitcast_dynamic-update-slice_fusion.2
  194.6 0.7 bitcast_dynamic-update-slice_fusion.2
  195.4 0.7 bitcast_dynamic-update-slice_fusion.2
  196.2 0.7 bitcast_dynamic-update-slice_fusion.2
  197.0 1.0 copy.51
  198.3 1.2 copy.52
  199.9 3.2 fusion.45
  203.1 3.1 fusion.54
  206.3 0.7 multiply_reduce_fusion
  207.0 0.9 fusion.29
  208.5 4.0 convolution_convert_fusion.1
  212.5 27.4 %all_to_all.15 = bf16[2,512,2048]{2,1,0:T(8,128)(2,1)S(1)} all-to-all(bf16[2,512,2048]{2,1,0:T(8,128)(2,1)S(1)} %bitcast.83), channel_id=1, replica_groups=mesh['rep'=2,'fs'=32,'tp'=2] {'tp'}, dimensions={0} | all-to-all | bytes 8388608 | tf_op jit(solution)/shard_map/all_to_all | solution.py:50
  239.8 1.0 convert_reduce_fusion.1
  241.4 0.7 fusion.10
  242.1 1.9 fusion.12
  244.3 0.8 pad_maximum_fusion.1
  245.1 1.1 dynamic-slice_reduce_fusion.2
  246.2 90.2 %all-gather.15.cloned.1.call-done = bf16[45056,64]{0,1:T(8,128)(2,1)} async-done(((bf16[1408,64]{0,1:T(8,128)(2,1)}), bf16[45056,64]{0,1:T(8,128)(2,1)}) %all-gather.15.cloned.1.call-update) | async-done | bytes 5767184 | tf_op jit(solution)/shard_map/all_gather | solution.py:190
  336.4 3.5 copy.55
  340.0 4.4 copy.49
  344.4 30.0 %all-gather.11.cloned.1.call-done = bf16[1024,2048]{1,0:T(8,128)(2,1)} async-done(((bf16[512,2048]{1,0:T(8,128)(2,1)}), bf16[1024,2048]{1,0:T(8,128)(2,1)}) %all-gather.11.cloned.1.call-update) | async-done | bytes 4194320 | tf_op jit(solution)/shard_map/all_gather | solution.py:175
  374.5 155.1 %all-gather.13.cloned.1.call-done = bf16[2048,2816]{1,0:T(8,128)(2,1)} async-done(((bf16[64,2816]{1,0:T(8,128)(2,1)}), bf16[2048,2816]{1,0:T(8,128)(2,1)}) %all-gather.13.cloned.1.call-update) | async-done | bytes 11534352 | tf_op jit(solution)/shard_map/all_gather | solution.py:17
  529.6 11.8 %fusion.17 = f32[1024,1408]{1,0:T(8,128)} fusion(bf16[1024,2048]{1,0:T(8,128)(2,1)} %all-gather.11.cloned.1.call-done, bf16[2048,2816]{1,0:T(8,128)(2,1)} %all-gather.13.cloned.1.call-done), kind=kOutput, calls=%fused_computation.26 | convolution fusion | flops 5908463616 | bytes 15728640 | tf_op jit(solution)/shard_map/dot_general | solution.py:178
  541.4 8.5 %fusion.23 = f32[1024,1408]{1,0:T(8,128)} fusion(bf16[1024,2048]{1,0:T(8,128)(2,1)S(1)} %copy-done.13, bf16[2048,2816]{1,0:T(8,128)(2,1)S(1)} %copy-done.11), kind=kOutput, calls=%fused_computation.28 | convolution fusion | flops 5908463616 | bytes 15728640 | tf_op jit(solution)/shard_map/dot_general | solution.py:179
  549.9 23.0 %convolution_convert_fusion = bf16[1024,2048]{1,0:T(8,128)(2,1)} fusion(bf16[1408,2048]{0,1:T(8,128)(2,1)} %bitcast.81, f32[1024,1408]{1,0:T(8,128)} %fusion.23, f32[1024,1408]{1,0:T(8,128)} %fusion.17, f32[1408]{0:T(1024)S(1)} %get-tuple-element.59, f32[1408]{0:T(1024)S(1)} %get-tuple-element.58, f32[1408]{0:T(1024)S(1)} %get-tuple-element.57, ...), kind=kOutput, calls=%fused_computation.29 | convolution fusion | flops 5930745856 | bytes 21529600 | tf_op jit(solution)/shard_map/dot_general | solution.py:192
  572.9 28.2 %all_to_all.16 = bf16[2,512,2048]{2,1,0:T(8,128)(2,1)S(1)} all-to-all(bf16[2,512,2048]{2,1,0:T(8,128)(2,1)} %bitcast.82), channel_id=1, replica_groups=mesh['rep'=2,'fs'=32,'tp'=2] {'tp'}, dimensions={0} | all-to-all | bytes 8388608 | tf_op jit(solution)/shard_map/all_to_all | solution.py:50
  601.1 1.0 convert_reduce_fusion
  602.1 2.1 fusion.13
  (78 shorter events, 5.7 us)
Async XLA Ops:
  6.5 5.7 copy-start.7
  6.5 5.7 copy-start.8
  6.5 5.7 copy-start.9
  6.5 6.4 %copy-start.6 = (bf16[512,64]{0,1:T(8,128)(2,1)S(1)}, bf16[512,64]{0,1:T(8,128)(2,1)}, u32[]{:S(2)}) copy-start(bf16[512,64]{0,1:T(8,128)(2,1)} %param.19) | copy-start | bytes 196612
  6.5 25.8 %all-gather.7.cloned.1.call-start = ((), (), s32[]{:S(2)}) async-start(), calls=%async_computation.3 | async-start | bytes 6291456 | tf_op jit(solution)/shard_map/all_gather | solution.py:147
  12.2 160.4 %all-gather.9.cloned.1.call-start = ((), (), s32[]{:S(2)}) async-start(), calls=%async_computation.4 | async-start | bytes 4325376 | tf_op jit(solution)/shard_map/all_gather | solution.py:17
  14.6 193.9 %all-to-all-start = ((bf16[32,512,64]{1,2,0:T(8,128)(2,1)}), bf16[32,512,64]{1,2,0:T(8,128)(2,1)}, u32[]{:S(2)}, u32[]{:S(2)}) async-start(bf16[32,512,64]{1,2,0:T(8,128)(2,1)} %broadcast_in_dim.25), calls=%async_computation | async-start | bytes 4194304 | tf_op jit(solution)/shard_map/all_to_all | solution.py:26
  23.9 312.5 %all-gather.15.cloned.1.call-start = ((), (), s32[]{:S(2)}) async-start(), calls=%async_computation.7 | async-start | bytes 5947392 | tf_op jit(solution)/shard_map/all_gather | solution.py:190
  24.6 349.8 %all-gather.11.cloned.1.call-start = ((), (), s32[]{:S(2)}) async-start(), calls=%async_computation.5 | async-start | bytes 6291456 | tf_op jit(solution)/shard_map/all_gather | solution.py:175
  172.6 4.1 copy-start.12
  189.2 0.8 copy-start.1
  198.3 4.8 copy-start.2
  199.9 3.2 copy-start.3
  239.8 1.6 copy-start
  241.4 0.7 copy-start.10
  242.1 2.2 copy-start.4
  242.1 2.2 copy-start.5
  244.0 285.5 %all-gather.13.cloned.1.call-start = ((), (), s32[]{:S(2)}) async-start(), calls=%async_computation.6 | async-start | bytes 11894784 | tf_op jit(solution)/shard_map/all_gather | solution.py:17
  529.5 11.8 %copy-start.11 = (bf16[2048,2816]{1,0:T(8,128)(2,1)S(1)}, bf16[2048,2816]{1,0:T(8,128)(2,1)}, u32[]{:S(2)}) copy-start(bf16[2048,2816]{1,0:T(8,128)(2,1)} %all-gather.13.cloned.1.call-done) | copy-start | bytes 34603012
  529.6 11.8 %copy-start.13 = (bf16[1024,2048]{1,0:T(8,128)(2,1)S(1)}, bf16[1024,2048]{1,0:T(8,128)(2,1)}, u32[]{:S(2)}) copy-start(bf16[1024,2048]{1,0:T(8,128)(2,1)} %all-gather.11.cloned.1.call-done) | copy-start | bytes 12582916
Sparse Core Ops, SparseCore 0:
  12.3 19.9 all-gather.6
  34.0 138.5 all-gather.8
  174.2 162.1 all-gather.14
  338.0 36.4 all-gather.10
  376.0 153.5 all-gather.12
